TPU v7x, 512 devices: a 4x2x32 block of a 4x8x32 slice. The times are simulated.
512 devices in a mesh: grp: 2 (over y), sp: 64 (over z, core), tp: 4 (over x).
Axes of the slice: x: 4, y: 2, z: 32, core: 2. Of those that a mesh axis runs over, the one named last changes fastest.
The devices are a block of a 4x8x32 slice.
Arguments:
- tokens: bfloat16 [49152, 2048], P(('grp', 'sp')), parts along dimension 0, may hold values from -6 to 6
- norm_gain: float32 [2, 2048], replicated, may hold values from 0.1 to 1.9
- entry_weight: bfloat16 [2, 2048, 2048], P(None, 'sp', 'tp'), may hold values from -0.125 to 0.125
- mix_weight: bfloat16 [2, 4, 512, 512], P(None, 'tp'), may hold values from -0.25 to 0.25
- pool_gain: float32 [2, 2048], P(None, 'tp'), may hold values from 0.1 to 1.9
- back_weight: bfloat16 [2, 2048, 2048], P(None, 'tp', 'sp'), may hold values from -0.25 to 0.25
Outputs:
- result_tokens: bfloat16 [49152, 2048], P(('grp', 'sp')), parts along dimension 0
There are 2 independent parts, one for each index of `grp`. A program takes and returns all parts, laid end to end along the dimension named above; an argument that names none is the same for every part. Nothing has to cross between parts.
All inputs are finite; a program needn't handle non-finite values.
Results may differ from a plain program's by a relative error of at most 0.018.
Values may be sent and summed in bfloat16 or wider, within the bound.
A program may use at most 64 MiB of HBM per device.

v0:
```python
import jax
import jax.numpy as jnp
from jax import lax
from jax.sharding import PartitionSpec as P

GROUPS = 4
LAYERS = 2
EPSILON = 1e-05


def extended_2(value, sides, width):
    for axis, dim in sides:
        size, length = (lax.axis_size(axis), value.shape[dim])
        up = [(i, (i + 1) % size) for i in range(size - 1)]
        down = [(j, i) for i, j in up]
        last = lax.slice_in_dim(value, length - width, length, axis=dim)
        first = lax.slice_in_dim(value, 0, width, axis=dim)
        before = lax.ppermute(last, axis, up)
        after = lax.ppermute(first, axis, down)
        value = jnp.concatenate([before, value, after], axis=dim)
    return value


def gather_turned(arrays, axis, dims):
    turned = [jnp.moveaxis(a, dim, 0) for a, dim in zip(arrays, dims)]
    both = jnp.concatenate([t.reshape(len(t), -1) for t in turned], axis=1)
    out, at, done = (lax.all_gather(both, axis, axis=0, tiled=True), 0, [])
    for t, dim in zip(turned, dims):
        section = out[:, at : at + t[0].size].reshape(-1, *t.shape[1:])
        done.append(jnp.moveaxis(section, 0, dim))
        at += t[0].size
    return tuple(done)


def from_everyone(value, axis):
    length = lax.axis_size(axis)
    return lax.all_to_all(
        jnp.broadcast_to(value[None], (length, *value.shape)), axis, 0, 0, tiled=True
    )


def over_copies(value, axis):
    everything = from_everyone(value, axis)
    return jnp.sum(everything.astype(jnp.float32), axis=0)


def window_mean(padded, positions, halves, total_length, reach):
    row_count = positions.shape[0]
    summed = jnp.zeros((row_count,) + padded.shape[1:], jnp.float32)
    for offset in range(-reach, reach):
        inside = ((offset >= -halves) & (offset < halves)).astype(jnp.float32)
        summed = (
            summed + padded[reach + offset : reach + offset + row_count] * inside[None, :, None]
        )
    lower = jnp.maximum(positions[:, None] - halves[None, :], 0)
    upper = jnp.minimum(positions[:, None] + halves[None, :], total_length)
    counted = (upper - lower).astype(jnp.float32)
    return summed / counted[:, :, None]


def normalize(state, gain):
    values = state.astype(jnp.float32)
    scaled = values * lax.rsqrt(jnp.mean(values * values, axis=-1, keepdims=True) + EPSILON)
    return (scaled * gain).astype(jnp.bfloat16)


def pool_groups(pooled_in, mix_layer, gain_layer, reach):
    row_count = pooled_in.shape[0]
    group_here = mix_layer.shape[0]
    width = mix_layer.shape[1]
    extended = extended_2(pooled_in, (("sp", 0),), reach)
    first_group = lax.axis_index("tp") * group_here
    halves = jnp.left_shift(jnp.int32(1), first_group + jnp.arange(group_here, dtype=jnp.int32))
    positions = lax.axis_index("sp") * row_count + jnp.arange(row_count, dtype=jnp.int32)
    total_length = lax.axis_size("sp") * row_count
    padded = extended.reshape(row_count + 2 * reach, group_here, width).astype(jnp.float32)
    means = window_mean(padded, positions, halves, total_length, reach)
    differ = (means - padded[reach : reach + row_count]).astype(jnp.bfloat16)
    mixed = jnp.einsum("tgc,gcd->tgd", differ, mix_layer, preferred_element_type=jnp.float32)
    return (mixed.reshape(row_count, group_here * width) * gain_layer).astype(jnp.bfloat16)


def per_device(tokens, norm_gain, entry_weight, mix_weight, pool_gain, back_weight):
    reach = 2 ** (GROUPS - 1)
    state = tokens
    entry_all, back_all = gather_turned((entry_weight, back_weight), "sp", (1, 2))
    for layer in range(LAYERS):
        normed = normalize(state, norm_gain[layer])
        pooled_in = jnp.dot(normed, entry_all[layer], preferred_element_type=jnp.float32).astype(
            jnp.bfloat16
        )
        back_local = back_all[layer]
        mixed = pool_groups(pooled_in, mix_weight[layer], pool_gain[layer], reach)
        update = jnp.dot(mixed, back_local, preferred_element_type=jnp.float32)
        summed = over_copies(update.astype(jnp.bfloat16), "tp").astype(jnp.float32)
        state = (state.astype(jnp.float32) + summed).astype(jnp.bfloat16)
    return state


def solution(mesh):
    return jax.shard_map(
        per_device,
        mesh=mesh,
        in_specs=(
            P(("grp", "sp"), None),
            P(),
            P(None, "sp", "tp"),
            P(None, "tp", None, None),
            P(None, "tp"),
            P(None, "tp", "sp"),
        ),
        out_specs=P(("grp", "sp"), None),
        check_vma=False,
    )
```

profile of v0, /device:TPU:33, one launch (start us, length us, event | category | flops | bytes accessed | tf_op | source)
XLA Modules:
  0.0 392.6 jit_solution(11383457933430418808)
XLA Ops:
  6.6 0.8 copy.17
  7.4 0.8 copy.18
  9.0 1.8 fusion
  12.4 164.7 %all-gather.2.cloned.1.call-done = bf16[2048,2048]{1,0:T(8,128)(2,1)} async-done(((bf16[32,2048]{1,0:T(8,128)(2,1)}), bf16[2048,2048]{1,0:T(8,128)(2,1)}) %all-gather.2.cloned.1.call-update) | async-done | bytes 8388624 | tf_op jit(solution)/shard_map/all_gather | solution.py:27
  177.1 5.2 %fusion.83 = (bf16[2048,1024]{1,0:T(8,128)(2,1)S(1)}, bf16[2048,1024]{1,0:T(8,128)(2,1)}) fusion(bf16[2048,2048]{1,0:T(8,128)(2,1)} %all-gather.2.cloned.1.call-done), kind=kLoop, calls=%fused_computation.119 | loop fusion | bytes 16777216 | tf_op jit(solution)/shard_map/slice | solution.py:29
  182.6 1.3 copy-done
  184.0 1.0 fusion.20
  185.0 2.0 collective-permute-start
  187.0 2.4 collective-permute-start.1
  189.5 6.6 %copy.15 = bf16[2048,1024]{0,1:T(8,128)(2,1)} copy(bf16[2048,1024]{1,0:T(8,128)(2,1)} %get-tuple-element.8) | data formatting | bytes 8388608 | tf_op jit(solution)/shard_map/reshape | solution.py:29
  196.1 1.0 maximum_convert_fusion
  197.1 11.0 %convolution_convert_fusion.1 = bf16[384,2048]{1,0:T(8,128)(2,1)S(1)} fusion(bf16[2,512,2048]{2,1,0:T(8,128)(2,1)} %bitcast.97, bf16[2,1,512,512]{3,2,1,0:T(8,128)(2,1)} %param.9, f32[512]{0:T(512)S(1)} %bitcast.112, f32[400,1,512]{2,0,1:T(8,128)} %maximum_convert_fusion, f32[384]{0:T(512)S(1)} %subtract_convert_fusion, f32[]{:T(128)S(6)} %mul.373, ...), kind=kOutput, calls=%fused_computation.18 | convolution fusion | flops 1014497280 | bytes 16780864 | tf_op jit(solution)/shard_map/dot_general | solution.py:94
  208.9 75.3 %all_to_all.10 = bf16[4,384,2048]{2,1,0:T(8,128)(2,1)S(1)} all-to-all(bf16[4,384,2048]{2,1,0:T(8,128)(2,1)S(1)} %broadcast_in_dim.4), channel_id=1, replica_groups=mesh['grp'=2,'sp'=64,'tp'=4] {'tp'}, dimensions={0} | all-to-all | bytes 12582912 | tf_op jit(solution)/shard_map/all_to_all | solution.py:37
  284.2 1.3 convert_reduce_fusion.1
  286.1 1.6 copy-done.2
  287.7 1.0 fusion.23
  288.7 3.5 collective-permute-start.2
  292.2 2.1 collective-permute-start.3
  294.4 2.9 collective-permute-done.3
  297.2 1.0 maximum_convert_fusion.1
  298.2 11.0 %convolution_convert_fusion = bf16[384,2048]{1,0:T(8,128)(2,1)S(1)} fusion(bf16[2,512,2048]{2,1,0:T(8,128)(2,1)} %bitcast.98, bf16[2,1,512,512]{3,2,1,0:T(8,128)(2,1)} %param.9, f32[512]{0:T(512)S(1)} %bitcast.111, f32[400,1,512]{2,0,1:T(8,128)} %maximum_convert_fusion.1, f32[384]{0:T(512)S(1)} %subtract_convert_fusion, f32[]{:T(128)S(6)} %mul.373, ...), kind=kOutput, calls=%fused_computation.17 | convolution fusion | flops 1014497280 | bytes 16780864 | tf_op jit(solution)/shard_map/dot_general | solution.py:94
  310.0 72.8 %all_to_all.11 = bf16[4,384,2048]{2,1,0:T(8,128)(2,1)S(1)} all-to-all(bf16[4,384,2048]{2,1,0:T(8,128)(2,1)S(1)} %broadcast_in_dim.5), channel_id=1, replica_groups=mesh['grp'=2,'sp'=64,'tp'=4] {'tp'}, dimensions={0} | all-to-all | bytes 12582912 | tf_op jit(solution)/shard_map/all_to_all | solution.py:37
  382.8 1.3 convert_reduce_fusion
  384.1 1.6 fusion.7
  (21 shorter events, 4.8 us)
Async XLA Ops:
  6.5 170.5 %all-gather.2.cloned.1.call-start = ((), (), s32[]{:S(2)}) async-start(), calls=%async_computation.2 | async-start | bytes 8519680 | tf_op jit(solution)/shard_map/all_gather | solution.py:27
  182.3 1.7 copy-start
  182.6 2.4 copy-start.1
  185.0 11.1 %collective-permute-start = (bf16[8,512]{1,0:T(8,128)(2,1)S(1)}, bf16[8,512]{1,0:T(8,128)(2,1)S(1)}, u32[]{:S(2)}, u32[]{:S(2)}) collective-permute-start(bf16[8,512]{1,0:T(8,128)(2,1)S(1)} %get-tuple-element.11), channel_id=1, source_target_pairs={{0,4},{4,8},{8,12},{12,16},{16,20},{20,24},{24,28},{28,32},{32,36}... | collective-permute-start | bytes 24584 | tf_op jit(solution)/shard_map/ppermute | solution.py:18
  187.0 9.1 %collective-permute-start.1 = (bf16[8,512]{1,0:T(8,128)(2,1)S(1)}, bf16[8,512]{1,0:T(8,128)(2,1)S(1)}, u32[]{:S(2)}, u32[]{:S(2)}) collective-permute-start(bf16[8,512]{1,0:T(8,128)(2,1)S(1)} %get-tuple-element.12), channel_id=1, source_target_pairs={{4,0},{8,4},{12,8},{16,12},{20,16},{24,20},{28,24},{32,28},{36,32}... | collective-permute-start | bytes 24584 | tf_op jit(solution)/shard_map/ppermute | solution.py:19
  285.5 2.2 copy-start.2
  288.7 5.6 %collective-permute-start.2 = (bf16[8,512]{1,0:T(8,128)(2,1)S(1)}, bf16[8,512]{1,0:T(8,128)(2,1)S(1)}, u32[]{:S(2)}, u32[]{:S(2)}) collective-permute-start(bf16[8,512]{1,0:T(8,128)(2,1)S(1)} %get-tuple-element.9), channel_id=1, source_target_pairs={{0,4},{4,8},{8,12},{12,16},{16,20},{20,24},{24,28},{28,32},{32,36}... | collective-permute-start | bytes 24584 | tf_op jit(solution)/shard_map/ppermute | solution.py:18
  292.2 5.0 %collective-permute-start.3 = (bf16[8,512]{1,0:T(8,128)(2,1)S(1)}, bf16[8,512]{1,0:T(8,128)(2,1)S(1)}, u32[]{:S(2)}, u32[]{:S(2)}) collective-permute-start(bf16[8,512]{1,0:T(8,128)(2,1)S(1)} %get-tuple-element.10), channel_id=1, source_target_pairs={{4,0},{8,4},{12,8},{16,12},{20,16},{24,20},{28,24},{32,28},{36,32}... | collective-permute-start | bytes 24584 | tf_op jit(solution)/shard_map/ppermute | solution.py:19
Sparse Core Ops, SparseCore 0:
  9.5 167.5 all-gather.1
where the time goes:
time: 393 us
  waiting for transfers between devices  168 us (43%)
  blocking collectives  148 us (38%)
  matrix products  24 us (6%)
  local copies, waits for them, and re-layouts  19.9 us (5%)
  between operations  13.7 us (3%)
  starting transfers between devices  9.98 us (3%)
  other arithmetic  9.18 us (2%)
    all_gather x1, waiting for transfers between devices, gather_turned(): out, at, done = (lax.all_gather(both, axis, axis=0, tiled=True), 0, [])  165 us
    all_to_all x2, blocking collectives, from_everyone(): lax.all_to_all(jnp.broadcast_to(value[None], (length, *value.shape)), axi...  148 us
    dot_general x2, matrix products, per_device(): update = jnp.dot(mixed, back_local, preferred_element_type=jnp.float32)  22 us
  transfers between devices with their start and end apart: 5, of which 2 were waited for; matrix products, arithmetic and copies ran while one was open for 3% of the time, Pallas kernels for 0%

commit v1 on v0

--- a/solution.py
+++ b/solution.py
@@ -6,6 +6,11 @@
 GROUPS = 4
 LAYERS = 2
 EPSILON = 1e-05
+
+
+def all_by_exchange(x, axis, along):
+    outgoing = jnp.stack([x] * lax.axis_size(axis))
+    return jnp.concatenate(lax.all_to_all(outgoing, axis, 0, 0), axis=along)
 
 
 def extended_2(value, sides, width):
@@ -24,7 +29,7 @@
 def gather_turned(arrays, axis, dims):
     turned = [jnp.moveaxis(a, dim, 0) for a, dim in zip(arrays, dims)]
     both = jnp.concatenate([t.reshape(len(t), -1) for t in turned], axis=1)
-    out, at, done = (lax.all_gather(both, axis, axis=0, tiled=True), 0, [])
+    out, at, done = (all_by_exchange(both, axis, 0), 0, [])
     for t, dim in zip(turned, dims):
         section = out[:, at : at + t[0].size].reshape(-1, *t.shape[1:])
         done.append(jnp.moveaxis(section, 0, dim))

time: 393 us -> 1010 us (2.57)
  waiting for transfers between devices: 168 us -> 728 us
  starting transfers between devices: 9.98 us -> 68.9 us
  between operations: 13.7 us -> 0.32 us
    all_to_all x0 -> x1, waiting for transfers between devices: none -> 726 us  [all_by_exchange(): return jnp.concatenate(lax.all_to_all(outgoing, axis, 0, 0), axis=along)]
    all_gather x1 -> x0, waiting for transfers between devices: 165 us -> none  [gather_turned(): out, at, done = (lax.all_gather(both, axis, axis=0, tiled=True), 0, [])]
    all_to_all x0 -> x1, starting transfers between devices: none -> 47.6 us  [all_by_exchange(): return jnp.concatenate(lax.all_to_all(outgoing, axis, 0, 0), axis=along)]
  transfers between devices with their start and end apart: 5 -> 5, of which waited for: 2 -> 2; matrix products, arithmetic and copies ran while one was open for 3% -> 1% of each run, Pallas kernels for 0% -> 0%
where the time goes in v1:
time: 1010 us
  waiting for transfers between devices  728 us (72%)
  blocking collectives  149 us (15%)
  starting transfers between devices  68.9 us (7%)
  local copies, waits for them, and re-layouts  28.2 us (3%)
  matrix products  24.9 us (2%)
    all_to_all x1, waiting for transfers between devices, all_by_exchange(): return jnp.concatenate(lax.all_to_all(outgoing, axis, 0, 0), axis=along)  726 us
    all_to_all x2, blocking collectives, from_everyone(): lax.all_to_all(jnp.broadcast_to(value[None], (length, *value.shape)), axi...  149 us
    all_to_all x1, starting transfers between devices, all_by_exchange(): return jnp.concatenate(lax.all_to_all(outgoing, axis, 0, 0), axis=along)  47.6 us
    dot_general x2, matrix products, per_device(): update = jnp.dot(mixed, back_local, preferred_element_type=jnp.float32)  21.2 us
  transfers between devices with their start and end apart: 5, of which 2 were waited for; matrix products, arithmetic and copies ran while one was open for 1% of the time, Pallas kernels for 0%

profile of v1, /device:TPU:33, one launch (start us, length us, event | category | flops | bytes accessed | tf_op | source)
XLA Modules:
  0.0 1006.6 jit_solution(559730007724326502)
XLA Ops:
  0.0 0.8 copy.23
  1.7 4.3 stack.2
  6.0 47.6 %all-to-all-start = ((bf16[64,32,2048]{2,1,0:T(8,128)(2,1)}), bf16[64,32,2048]{2,1,0:T(8,128)(2,1)}, u32[]{:S(2)}, u32[]{:S(2)}) async-start(bf16[64,32,2048]{2,1,0:T(8,128)(2,1)} %stack.2), calls=%async_computation | async-start | bytes 16777216 | tf_op jit(solution)/shard_map/all_to_all | solution.py:13
  54.0 725.9 %all-to-all-done = bf16[64,32,2048]{2,1,0:T(8,128)(2,1)} async-done(((bf16[64,32,2048]{2,1,0:T(8,128)(2,1)}), bf16[64,32,2048]{2,1,0:T(8,128)(2,1)}, u32[]{:S(2)}, u32[]{:S(2)}) %all-to-all-start) | async-done | bytes 8388640 | tf_op jit(solution)/shard_map/all_to_all | solution.py:13
  779.9 5.9 fusion.83
  785.8 6.5 copy.18
  792.4 2.6 fusion.20
  795.0 13.5 %collective-permute-start = (bf16[8,512]{1,0:T(8,128)(2,1)S(1)}, bf16[8,512]{1,0:T(8,128)(2,1)S(1)}, u32[]{:S(2)}, u32[]{:S(2)}) collective-permute-start(bf16[8,512]{1,0:T(8,128)(2,1)S(1)} %get-tuple-element.11), channel_id=1, source_target_pairs={{0,4},{4,8},{8,12},{12,16},{16,20},{20,24},{24,28},{28,32},{32,36}... | collective-permute-start | bytes 24584 | tf_op jit(solution)/shard_map/ppermute | solution.py:23
  808.5 3.2 collective-permute-start.1
  811.9 6.5 copy.22
  818.4 1.0 maximum_convert_fusion
  819.4 10.6 %convolution_convert_fusion.1 = bf16[384,2048]{1,0:T(8,128)(2,1)S(1)} fusion(bf16[2,512,2048]{2,1,0:T(8,128)(2,1)} %bitcast.95, bf16[2,1,512,512]{3,2,1,0:T(8,128)(2,1)} %param.9, f32[512]{0:T(512)S(1)} %bitcast.110, f32[400,1,512]{2,0,1:T(8,128)} %maximum_convert_fusion, f32[384]{0:T(512)S(1)} %subtract_convert_fusion, f32[]{:T(128)S(6)} %mul.373, ...), kind=kOutput, calls=%fused_computation.17 | convolution fusion | flops 1014497280 | bytes 16780864 | tf_op jit(solution)/shard_map/dot_general | solution.py:99
  830.8 75.7 %all_to_all.15 = bf16[4,384,2048]{2,1,0:T(8,128)(2,1)S(1)} all-to-all(bf16[4,384,2048]{2,1,0:T(8,128)(2,1)S(1)} %broadcast_in_dim.4), channel_id=1, replica_groups=mesh['grp'=2,'sp'=64,'tp'=4] {'tp'}, dimensions={0} | all-to-all | bytes 12582912 | tf_op jit(solution)/shard_map/all_to_all | solution.py:42
  906.5 1.3 convert_reduce_fusion.1
  908.3 1.6 copy-done.1
  910.0 1.0 fusion.23
  911.0 2.0 collective-permute-start.2
  913.0 2.6 collective-permute-start.3
  915.6 2.4 collective-permute-done.3
  918.0 1.0 maximum_convert_fusion.1
  919.0 10.7 %convolution_convert_fusion = bf16[384,2048]{1,0:T(8,128)(2,1)S(1)} fusion(bf16[2,512,2048]{2,1,0:T(8,128)(2,1)} %bitcast.96, bf16[2,1,512,512]{3,2,1,0:T(8,128)(2,1)} %param.9, f32[512]{0:T(512)S(1)} %bitcast.109, f32[400,1,512]{2,0,1:T(8,128)} %maximum_convert_fusion.1, f32[384]{0:T(512)S(1)} %subtract_convert_fusion, f32[]{:T(128)S(6)} %mul.373, ...), kind=kOutput, calls=%fused_computation.16 | convolution fusion | flops 1014497280 | bytes 16780864 | tf_op jit(solution)/shard_map/dot_general | solution.py:99
  930.4 73.3 %all_to_all.16 = bf16[4,384,2048]{2,1,0:T(8,128)(2,1)S(1)} all-to-all(bf16[4,384,2048]{2,1,0:T(8,128)(2,1)S(1)} %broadcast_in_dim.5), channel_id=1, replica_groups=mesh['grp'=2,'sp'=64,'tp'=4] {'tp'}, dimensions={0} | all-to-all | bytes 12582912 | tf_op jit(solution)/shard_map/all_to_all | solution.py:42
  1003.7 1.3 convert_reduce_fusion
  1005.0 1.6 fusion.7
  (23 shorter events, 3.4 us)
Async XLA Ops:
  6.0 47.6 %copy-start = (bf16[384,2048]{1,0:T(8,128)(2,1)S(1)}, bf16[384,2048]{1,0:T(8,128)(2,1)}, u32[]{:S(2)}) copy-start(bf16[384,2048]{1,0:T(8,128)(2,1)} %param.6) | copy-start | bytes 4718596
  6.0 48.0 %copy-start.3 = (f32[2,512]{1,0:T(2,128)S(1)}, f32[2,512]{1,0:T(2,128)}, u32[]{:S(2)}) copy-start(f32[2,512]{1,0:T(2,128)} %param.10) | copy-start | bytes 12292
  6.0 48.0 %copy-start.2 = (f32[2,2048]{1,0:T(2,128)S(1)}, f32[2,2048]{1,0:T(2,128)}, u32[]{:S(2)}) copy-start(f32[2,2048]{1,0:T(2,128)} %param.7) | copy-start | bytes 49156
  6.0 773.9 %all-to-all-start = ((bf16[64,32,2048]{2,1,0:T(8,128)(2,1)}), bf16[64,32,2048]{2,1,0:T(8,128)(2,1)}, u32[]{:S(2)}, u32[]{:S(2)}) async-start(bf16[64,32,2048]{2,1,0:T(8,128)(2,1)} %stack.2), calls=%async_computation | async-start | bytes 16777216 | tf_op jit(solution)/shard_map/all_to_all | solution.py:13
  795.0 23.4 %collective-permute-start = (bf16[8,512]{1,0:T(8,128)(2,1)S(1)}, bf16[8,512]{1,0:T(8,128)(2,1)S(1)}, u32[]{:S(2)}, u32[]{:S(2)}) collective-permute-start(bf16[8,512]{1,0:T(8,128)(2,1)S(1)} %get-tuple-element.11), channel_id=1, source_target_pairs={{0,4},{4,8},{8,12},{12,16},{16,20},{20,24},{24,28},{28,32},{32,36}... | collective-permute-start | bytes 24584 | tf_op jit(solution)/shard_map/ppermute | solution.py:23
  808.5 9.9 collective-permute-start.1
  907.8 2.2 copy-start.1
  911.0 4.6 collective-permute-start.2
  913.0 5.0 collective-permute-start.3
